TPU v7x, 128 devices: a whole 4x4x4 slice. The times are simulated.
128 devices in a mesh: fs: 16 (over z, y), tp: 8 (over x, core).
Axes of the slice: x: 4, y: 4, z: 4, core: 2. Of those that a mesh axis runs over, the one named last changes fastest.
Arguments:
- resid: bfloat16 [24576, 2048], P(('fs', 'tp')), may hold values from -6 to 6
- norm1_gain: float32 [2048], replicated, may hold values from 0.1 to 1.9
- w_value: float32 [2048, 2048], P('fs', 'tp'), may hold values from -0.125 to 0.125
- w_gate: float32 [2048, 2048], P('fs', 'tp'), may hold values from -0.125 to 0.125
- value_scale: float32 [2048], replicated, may hold values from 0.3 to 3
- gate_scale: float32 [2048], replicated, may hold values from 0.5 to 3
- conv_taps: float32 [31, 2048], replicated, may hold values from -1 to 1
- conv_gain: float32 [2048], replicated, may hold values from 0.1 to 1.9
- w_point: float32 [2048, 2048], P('tp', 'fs'), may hold values from -0.125 to 0.125
- point_scale: float32 [2048], P('fs'), may hold values from 0.5 to 3
- norm2_gain: float32 [2048], replicated, may hold values from 0.1 to 1.9
- w_up: float32 [2048, 8192], P('fs', 'tp'), may hold values from -0.125 to 0.125
- up_scale: float32 [8192], P('tp'), may hold values from 0.5 to 1.5
- w_down: float32 [8192, 2048], P('tp', 'fs'), may hold values from -0.0625 to 0.0625
- down_scale: float32 [2048], P('fs'), may hold values from 0.3 to 1
Outputs:
- layer_out: bfloat16 [24576, 2048], P(('fs', 'tp'))
All inputs are finite; a program needn't handle non-finite values.
Results may differ from a plain program's by a relative error of at most 0.015.
Values may be sent and summed in bfloat16 or wider, within the bound.
A program may use at most 128 MiB of HBM per device.

v0:
```python
import jax
import jax.numpy as jnp
from jax import lax
from jax.sharding import PartitionSpec as P

GROUPS = 4


def gather_turned(arrays, axis, dims):
    turned = [jnp.moveaxis(a, dim, 0) for a, dim in zip(arrays, dims)]
    both = jnp.concatenate([t.reshape(len(t), -1) for t in turned], axis=1)
    result, at, done = (lax.all_gather(both, axis, axis=0, tiled=True), 0, [])
    for t, dim in zip(turned, dims):
        slab = result[:, at : at + t[0].size].reshape(-1, *t.shape[1:])
        done.append(jnp.moveaxis(slab, 0, dim))
        at += t[0].size
    return tuple(done)


def laid_out(pieces, dim):
    shape = list(pieces.shape[1:])
    shape[dim] *= pieces.shape[0]
    return jnp.moveaxis(pieces, 0, dim).reshape(shape)


def from_everyone(x, axis):
    copies = jnp.broadcast_to(x, (lax.axis_size(axis), *x.shape))
    return lax.all_to_all(copies, axis, split_axis=0, concat_axis=0, tiled=True)


def gather_directly(x, axis, dim):
    return laid_out(from_everyone(x, axis), dim)


def over_copies(x, axis):
    return from_everyone(x, axis).sum(axis=0)


def in_one(arrays, axis):
    ends = [0]
    for a in arrays:
        ends.append(ends[-1] + a.size)
    running = over_copies(jnp.concatenate([a.ravel() for a in arrays]), axis)
    return tuple((running[b:e].reshape(a.shape) for a, b, e in zip(arrays, ends, ends[1:])))


def rms_scaled(values, gain):
    data = values.astype(jnp.float32)
    return data * lax.rsqrt(jnp.mean(data * data, axis=-1, keepdims=True) + 1e-06) * gain


def depthwise(padded, taps, length):
    wide = padded.astype(jnp.float32)
    conv = jnp.zeros((length, wide.shape[1]), jnp.float32)
    for offset in range(taps.shape[0]):
        conv = conv + taps[offset] * wide[offset : offset + length]
    return conv


def fetch_mlp(up_bf, down_bf):
    return gather_turned((up_bf, down_bf), "fs", (0, 1))


def shards(
    resid,
    norm1_gain,
    w_value,
    w_gate,
    value_scale,
    gate_scale,
    conv_taps,
    conv_gain,
    w_point,
    point_scale,
    norm2_gain,
    w_up,
    up_scale,
    w_down,
    down_scale,
):
    tok_rows = resid.shape[0]
    tp_count = lax.axis_size("tp")
    tp_rank = lax.axis_index("tp")
    seq_len = tok_rows * tp_count
    channels = value_scale.shape[0]
    group_width = channels // GROUPS
    reach = conv_taps.shape[0] // 2
    value_bf = w_value.astype(jnp.bfloat16)
    gate_bf = w_gate.astype(jnp.bfloat16)
    point_bf = w_point.astype(jnp.bfloat16)
    up_bf = w_up.astype(jnp.bfloat16)
    down_bf = w_down.astype(jnp.bfloat16)
    point_full, down_full = gather_turned((point_scale, down_scale), "fs", (0, 0))
    normed = rms_scaled(resid, norm1_gain).astype(jnp.bfloat16)
    value_rows, gate_rows, point_rows = gather_turned(
        (value_bf, gate_bf, point_bf), "fs", (0, 0, 1)
    )
    own_width = value_rows.shape[1]
    first = tp_rank * own_width
    own_value_scale = lax.dynamic_slice_in_dim(value_scale, first, own_width, 0)
    own_gate_scale = lax.dynamic_slice_in_dim(gate_scale, first, own_width, 0)
    own_taps = lax.dynamic_slice_in_dim(conv_taps, first, own_width, 1)
    own_gain = lax.dynamic_slice_in_dim(conv_gain, first, own_width, 0)
    piece = gather_directly(normed, "tp", 0)
    value = jnp.dot(piece, value_rows, preferred_element_type=jnp.float32) * own_value_scale
    gate = jnp.dot(piece, gate_rows, preferred_element_type=jnp.float32) * own_gate_scale
    glu_seq = (value * jax.nn.sigmoid(gate)).astype(jnp.bfloat16)
    padded = jnp.pad(glu_seq, ((reach, reach), (0, 0)))
    conv = depthwise(padded, own_taps, seq_len)
    member = ((first + jnp.arange(own_width)) % GROUPS)[:, None] == jnp.arange(GROUPS)[None, :]
    member = member.astype(jnp.float32)
    sums = jnp.dot(conv, member, precision=lax.Precision.HIGHEST)
    squares = jnp.dot(conv * conv, member, precision=lax.Precision.HIGHEST)
    totals, square_totals = in_one((sums, squares), "tp")
    gmean = jnp.dot(totals / group_width, member.T, precision=lax.Precision.HIGHEST)
    gsquare = jnp.dot(square_totals / group_width, member.T, precision=lax.Precision.HIGHEST)
    scaled = (conv - gmean) * lax.rsqrt(gsquare - gmean * gmean + 1e-05) * own_gain
    act = jax.nn.silu(scaled).astype(jnp.bfloat16)
    mixed = lax.psum_scatter(
        jnp.dot(act, point_rows, preferred_element_type=jnp.float32) * point_full,
        "tp",
        scatter_dimension=0,
        tiled=True,
    )
    middle = (resid.astype(jnp.float32) + mixed).astype(jnp.bfloat16)
    normed2 = rms_scaled(middle, norm2_gain).astype(jnp.bfloat16)
    up_cols, down_part = fetch_mlp(up_bf, down_bf)
    upper = (
        jnp.dot(gather_directly(normed2, "tp", 0), up_cols, preferred_element_type=jnp.float32)
        * up_scale
    )
    hidden = jnp.square(jax.nn.relu(upper)).astype(jnp.bfloat16)
    total = lax.psum_scatter(
        (jnp.dot(hidden, down_part, preferred_element_type=jnp.float32) * down_full).astype(
            jnp.bfloat16
        ),
        "tp",
        scatter_dimension=0,
        tiled=True,
    ).astype(jnp.float32)
    return (middle.astype(jnp.float32) + total).astype(jnp.bfloat16)


def solution(mesh):
    in_specs = (
        P(("fs", "tp"), None),
        P(),
        P("fs", "tp"),
        P("fs", "tp"),
        P(),
        P(),
        P(),
        P(),
        P("tp", "fs"),
        P("fs"),
        P(),
        P("fs", "tp"),
        P("tp"),
        P("tp", "fs"),
        P("fs"),
    )
    out_specs = P(("fs", "tp"), None)
    return jax.shard_map(shards, mesh=mesh, in_specs=in_specs, out_specs=out_specs, check_vma=False)
```

profile of v0, /device:TPU:1, one launch (start us, length us, event | category | flops | bytes accessed | tf_op | source)
XLA Modules:
  0.0 365.7 jit_solution(16230646207649153275)
XLA Ops:
  6.5 0.0 copy-start
  6.5 0.0 copy-start.3
  6.5 0.0 all-gather.3.cloned.1.call-start
  6.5 1.0 convert_bitcast_fusion.1
  7.5 1.0 copy.29
  8.5 1.0 copy.30
  9.6 0.7 pad_maximum_fusion.1
  10.3 0.0 all-gather.3.cloned.1.call-update
  10.3 0.0 copy-done
  10.3 0.2 fusion.16
  10.5 0.0 copy-done.3
  10.6 0.3 fusion.18
  10.8 3.5 broadcast_in_dim.6
  14.3 0.0 copy-start.5
  14.3 6.2 %all-to-all-start = ((bf16[8,192,2048]{2,1,0:T(8,128)(2,1)}), bf16[8,192,2048]{2,1,0:T(8,128)(2,1)}, u32[]{:S(2)}, u32[]{:S(2)}) async-start(bf16[8,192,2048]{2,1,0:T(8,128)(2,1)} %broadcast_in_dim.6), calls=%async_computation | async-start | bytes 12582912 | tf_op jit(solution)/shard_map/all_to_all | solution.py:28
  20.4 0.8 dynamic_slice.14
  21.2 0.8 dynamic_slice.13
  22.0 0.8 dynamic_slice.15
  22.7 0.0 copy-done.5
  22.7 0.0 copy-done.6
  22.7 21.5 %all_gather.10 = f32[2048,2]{0,1:T(2,128)S(1)} all-gather(f32[128,2]{0,1:T(2,128)S(1)} %pad_maximum_fusion.3), channel_id=1, replica_groups=mesh['fs'=16,'tp'=8] {'fs'}, dimensions={0}, use_global_device_ids=true | all-gather | bytes 17408 | tf_op jit(solution)/shard_map/all_gather | solution.py:12
  44.2 1.1 fusion.68
  45.3 1.2 constant_dynamic-slice_fusion
  46.5 45.2 %all-to-all-done = bf16[8,192,2048]{2,1,0:T(8,128)(2,1)} async-done(((bf16[8,192,2048]{2,1,0:T(8,128)(2,1)}), bf16[8,192,2048]{2,1,0:T(8,128)(2,1)}, u32[]{:S(2)}, u32[]{:S(2)}) %all-to-all-start) | async-done | bytes 6291488 | tf_op jit(solution)/shard_map/all_to_all | solution.py:28
  91.7 5.0 %fusion.14 = f32[1536,256]{1,0:T(8,128)S(1)} fusion(bf16[1536,2048]{1,0:T(8,128)(2,1)} %bitcast.1, bf16[2048,768]{0,1:T(8,128)(2,1)} %all-gather.3.cloned.1.call-done, f32[256]{0:T(256)S(1)} %dynamic_slice.14), kind=kOutput, calls=%fused_computation.18 | convolution fusion | flops 1612185600 | bytes 8913920 | tf_op jit(solution)/shard_map/dot_general | solution.py:106
  96.7 4.9 %fusion.15 = bf16[1536,256]{1,0:T(8,128)(2,1)S(1)} fusion(f32[1536,256]{1,0:T(8,128)S(1)} %fusion.14, bf16[1536,2048]{1,0:T(8,128)(2,1)} %bitcast.1, bf16[2048,768]{0,1:T(8,128)(2,1)} %all-gather.3.cloned.1.call-done, f32[256]{0:T(256)S(1)} %dynamic_slice.13), kind=kOutput, calls=%fused_computation.19 | convolution fusion | flops 1611792384 | bytes 9700352 | tf_op jit(solution)/shard_map/dot_general | solution.py:105
  101.6 0.2 pad_convert_fusion
  101.7 6.0 %fusion.24 = f32[1536,256]{1,0:T(8,128)S(1)} fusion(f32[1566,256]{1,0:T(8,128)S(1)} %pad_convert_fusion, f32[256]{0:T(256)S(1)} %bitcast.62, f32[256]{0:T(256)S(1)} %bitcast.64, f32[256]{0:T(256)S(1)} %bitcast.65, f32[256]{0:T(256)S(1)} %bitcast.66, f32[256]{0:T(256)S(1)} %bitcast.67, f32[256]{0:T(256)S(1)} %bitcast.68, f32[256]{0:T(256)S(1)} %bitcast.69, ...), kind=kLoop, calls=%fused_computation.35 | loop fusion | flops 23986176 | bytes 50363392 | tf_op jit(solution)/shard_map/add | solution.py:56
  107.8 1.8 fusion.60
  109.6 0.9 fusion.54
  110.5 1.6 reshape.84
  112.1 0.4 reshape.85
  112.5 0.9 broadcast_in_dim.7
  113.4 4.3 %all-to-all-start.1 = ((f32[8,1,12288]{2,1,0:T(1,128)}), f32[8,1,12288]{2,1,0:T(1,128)S(1)}, u32[]{:S(2)}, u32[]{:S(2)}) async-start(f32[8,1,12288]{2,1,0:T(1,128)} %broadcast_in_dim.7), calls=%async_computation.1 | async-start | bytes 786432 | tf_op jit(solution)/shard_map/all_to_all | solution.py:28
  117.8 0.0 reduce-scatter.3.cloned.1.call-start
  117.8 7.7 %all-to-all-done.1 = f32[8,1,12288]{2,1,0:T(1,128)S(1)} async-done(((f32[8,1,12288]{2,1,0:T(1,128)}), f32[8,1,12288]{2,1,0:T(1,128)S(1)}, u32[]{:S(2)}, u32[]{:S(2)}) %all-to-all-start.1) | async-done | bytes 393248 | tf_op jit(solution)/shard_map/all_to_all | solution.py:28
  125.5 0.3 reduce_sum.28
  125.8 0.8 div.26
  126.6 2.0 fusion.59
  128.6 0.8 div.28
  129.4 2.7 multiply_convert_fusion.2
  132.2 7.6 %convolution_multiply_fusion = f32[1536,2048]{1,0:T(8,128)} fusion(bf16[1536,256]{1,0:T(8,128)(2,1)S(1)} %multiply_convert_fusion.2, f32[2048]{0:T(1024)S(1)} %bitcast.48, bf16[2048,768]{0,1:T(8,128)(2,1)} %all-gather.3.cloned.1.call-done), kind=kOutput, calls=%fused_computation.1 | convolution fusion | flops 1613758464 | bytes 14426112 | tf_op jit(solution)/shard_map/dot_general | solution.py:120
  139.7 0.0 reduce-scatter.3.cloned.1.call-update
  139.7 0.0 all-gather.5.cloned.1.call-start
  139.8 1.0 copy-done.1
  140.7 0.2 copy.34
  140.9 0.0 copy-done.2
  141.0 0.8 pad_maximum_fusion
  141.8 0.0 all-gather.5.cloned.1.call-update
  141.8 0.0 copy-start.4
  141.8 71.1 %reduce-scatter.3.cloned.1.call-done = f32[192,2048]{1,0:T(8,128)} async-done(((f32[1536,2048]{1,0:T(8,128)}), f32[192,2048]{1,0:T(8,128)}) %reduce-scatter.3.cloned.1.call-update) | async-done | bytes 1572880 | tf_op jit(solution)/shard_map/reduce_scatter | solution.py:119
  212.9 1.7 fusion.20
  214.6 0.0 copy-done.4
  214.6 0.3 fusion.22
  214.9 3.5 broadcast_in_dim.8
  218.4 6.0 %all-to-all-start.2 = ((bf16[8,192,2048]{2,1,0:T(8,128)(2,1)}), bf16[8,192,2048]{2,1,0:T(8,128)(2,1)}, u32[]{:S(2)}, u32[]{:S(2)}) async-start(bf16[8,192,2048]{2,1,0:T(8,128)(2,1)} %broadcast_in_dim.8), calls=%async_computation.3 | async-start | bytes 12582912 | tf_op jit(solution)/shard_map/all_to_all | solution.py:28
  224.3 0.0 reduce-scatter.5.cloned.1.call-start
  224.3 66.9 %all-gather.5.cloned.1.call-done = bf16[2048,2048]{0,1:T(8,128)(2,1)} async-done(((bf16[128,2048]{0,1:T(8,128)(2,1)}), bf16[2048,2048]{0,1:T(8,128)(2,1)}) %all-gather.5.cloned.1.call-update) | async-done | bytes 8388624 | tf_op jit(solution)/shard_map/all_gather | solution.py:12
  291.2 4.4 %all-to-all-done.2 = bf16[8,192,2048]{2,1,0:T(8,128)(2,1)} async-done(((bf16[8,192,2048]{2,1,0:T(8,128)(2,1)}), bf16[8,192,2048]{2,1,0:T(8,128)(2,1)}, u32[]{:S(2)}, u32[]{:S(2)}) %all-to-all-start.2) | async-done | bytes 6291488 | tf_op jit(solution)/shard_map/all_to_all | solution.py:28
  295.6 0.0 copy-done.7
  295.6 19.4 %multiply_convert_fusion = bf16[1536,2048]{1,0:T(8,128)(2,1)} fusion(f32[2048]{0:T(1024)S(1)} %bitcast.49, bf16[2048,2048]{0,1:T(8,128)(2,1)} %all-gather.5.cloned.1.call-done, bf16[1536,2048]{1,0:T(8,128)(2,1)} %bitcast.36, f32[1024]{0:T(1024)S(1)} %copy-done.7), kind=kOutput, calls=%fused_computation | convolution fusion | flops 12897484800 | bytes 20983808 | tf_op jit(solution)/shard_map/dot_general | solution.py:134
  315.0 0.0 reduce-scatter.5.cloned.1.call-update
  315.1 41.8 %reduce-scatter.5.cloned.1.call-done = bf16[192,2048]{1,0:T(8,128)(2,1)} async-done(((bf16[1536,2048]{1,0:T(8,128)(2,1)}), bf16[192,2048]{1,0:T(8,128)(2,1)}) %reduce-scatter.5.cloned.1.call-update) | async-done | bytes 786448 | tf_op jit(solution)/shard_map/reduce_scatter | solution.py:133
  356.9 2.3 fusion.23
  (13 shorter events, 0.1 us)
Async XLA Ops:
  6.5 3.8 %copy-start = (bf16[192,2048]{1,0:T(8,128)(2,1)S(1)}, bf16[192,2048]{1,0:T(8,128)(2,1)}, u32[]{:S(2)}) copy-start(bf16[192,2048]{1,0:T(8,128)(2,1)} %param.15) | copy-start | bytes 2359300
  6.5 4.0 %copy-start.3 = (f32[2048]{0:T(1024)S(1)}, f32[2048]{0:T(1024)}, u32[]{:S(2)}) copy-start(f32[2048]{0:T(1024)} %param.16) | copy-start | bytes 24580
  6.5 85.2 %all-gather.3.cloned.1.call-start = ((), (), s32[]{:S(2)}) async-start(), calls=%async_computation.5 | async-start | bytes 3342336 | tf_op jit(solution)/shard_map/all_gather | solution.py:12
  14.3 8.4 %copy-start.5 = (f32[128]{0:T(128)S(1)}, f32[128]{0:T(128)}, u32[]{:S(2)}) copy-start(f32[128]{0:T(128)} %param.29) | copy-start | bytes 1540
  14.3 8.4 %copy-start.6 = (f32[128]{0:T(128)S(1)}, f32[128]{0:T(128)}, u32[]{:S(2)}) copy-start(f32[128]{0:T(128)} %param.24) | copy-start | bytes 1540
  14.3 77.4 %all-to-all-start = ((bf16[8,192,2048]{2,1,0:T(8,128)(2,1)}), bf16[8,192,2048]{2,1,0:T(8,128)(2,1)}, u32[]{:S(2)}, u32[]{:S(2)}) async-start(bf16[8,192,2048]{2,1,0:T(8,128)(2,1)} %broadcast_in_dim.6), calls=%async_computation | async-start | bytes 12582912 | tf_op jit(solution)/shard_map/all_to_all | solution.py:28
  113.4 12.0 %all-to-all-start.1 = ((f32[8,1,12288]{2,1,0:T(1,128)}), f32[8,1,12288]{2,1,0:T(1,128)S(1)}, u32[]{:S(2)}, u32[]{:S(2)}) async-start(f32[8,1,12288]{2,1,0:T(1,128)} %broadcast_in_dim.7), calls=%async_computation.1 | async-start | bytes 786432 | tf_op jit(solution)/shard_map/all_to_all | solution.py:28
  117.8 95.2 %reduce-scatter.3.cloned.1.call-start = ((), (), s32[]{:S(2)}) async-start(), calls=%async_computation.6 | async-start | bytes 14155776 | tf_op jit(solution)/shard_map/reduce_scatter | solution.py:119
  139.7 1.0 copy-start.1
  139.7 1.2 copy-start.2
  139.7 151.5 %all-gather.5.cloned.1.call-start = ((), (), s32[]{:S(2)}) async-start(), calls=%async_computation.7 | async-start | bytes 8912896 | tf_op jit(solution)/shard_map/all_gather | solution.py:12
  141.8 72.8 %copy-start.4 = (f32[2048]{0:T(1024)S(1)}, f32[2048]{0:T(1024)}, u32[]{:S(2)}) copy-start(f32[2048]{0:T(1024)} %param.25) | copy-start | bytes 24580
  218.4 77.2 %copy-start.7 = (f32[1024]{0:T(1024)S(1)}, f32[1024]{0:T(1024)}, u32[]{:S(2)}) copy-start(f32[1024]{0:T(1024)} %param.27) | copy-start | bytes 12292
  218.4 77.2 %all-to-all-start.2 = ((bf16[8,192,2048]{2,1,0:T(8,128)(2,1)}), bf16[8,192,2048]{2,1,0:T(8,128)(2,1)}, u32[]{:S(2)}, u32[]{:S(2)}) async-start(bf16[8,192,2048]{2,1,0:T(8,128)(2,1)} %broadcast_in_dim.8), calls=%async_computation.3 | async-start | bytes 12582912 | tf_op jit(solution)/shard_map/all_to_all | solution.py:28
  224.3 132.6 %reduce-scatter.5.cloned.1.call-start = ((), (), s32[]{:S(2)}) async-start(), calls=%async_computation.8 | async-start | bytes 7077888 | tf_op jit(solution)/shard_map/reduce_scatter | solution.py:133
Sparse Core Ops, SparseCore 0:
  10.4 53.8 all-gather.2
  139.9 73.0 reduce-scatter.2
  215.0 76.1 all-gather.4
  315.2 41.6 reduce-scatter.4
where the time goes:
time: 367 us; the launch traced here: 366 us
  waiting for transfers between devices  237 us (65%)
  matrix products  44.3 us (12%)
  blocking collectives  21.5 us (6%)
  local copies, waits for them, and re-layouts  19.2 us (5%)
  starting transfers between devices  16.5 us (4%)
  other arithmetic  13.8 us (4%)
  between operations  13.3 us (4%)
    reduce_scatter x1, waiting for transfers between devices, shards(): lax.psum_scatter(jnp.dot(act, point_rows, preferred_element_type=jnp.floa...  71.1 us
    all_gather x2, waiting for transfers between devices, gather_turned(): result, at, done = (lax.all_gather(both, axis, axis=0, tiled=True), 0, [])  66.9 us
    all_to_all x3, waiting for transfers between devices, from_everyone(): return lax.all_to_all(copies, axis, split_axis=0, concat_axis=0, tiled=True)  57.3 us
    reduce_scatter x1, waiting for transfers between devices, shards(): lax.psum_scatter((jnp.dot(hidden, down_part, preferred_element_type=jnp.f...  41.8 us
    all_gather x1, blocking collectives, gather_turned(): result, at, done = (lax.all_gather(both, axis, axis=0, tiled=True), 0, [])  21.5 us
    dot_general x1, matrix products, shards(): jnp.dot(hidden, down_part, preferred_element_type=jnp.float32) * down_full  19.4 us
    all_to_all x3, starting transfers between devices, from_everyone(): return lax.all_to_all(copies, axis, split_axis=0, concat_axis=0, tiled=True)  16.4 us
    broadcast_in_dim x3, local copies, waits for them, and re-layouts, from_everyone(): copies = jnp.broadcast_to(x, (lax.axis_size(axis), *x.shape))  7.88 us
  transfers between devices with their start and end apart: 7, of which 6 were waited for; matrix products, arithmetic and copies ran while one was open for 4% of the time, Pallas kernels for 0%

commit v1 on v0

--- a/solution.py
+++ b/solution.py
@@ -6,10 +6,17 @@
 GROUPS = 4
 
 
+def exchange_gather(shard, name, d):
+    peers = lax.axis_size(name)
+    blocks = jnp.stack([shard for _ in range(peers)])
+    blocks = lax.all_to_all(blocks, name, split_axis=0, concat_axis=0)
+    return jnp.concatenate(blocks, axis=d)
+
+
 def gather_turned(arrays, axis, dims):
     turned = [jnp.moveaxis(a, dim, 0) for a, dim in zip(arrays, dims)]
     both = jnp.concatenate([t.reshape(len(t), -1) for t in turned], axis=1)
-    result, at, done = (lax.all_gather(both, axis, axis=0, tiled=True), 0, [])
+    result, at, done = (exchange_gather(both, axis, 0), 0, [])
     for t, dim in zip(turned, dims):
         slab = result[:, at : at + t[0].size].reshape(-1, *t.shape[1:])
         done.append(jnp.moveaxis(slab, 0, dim))

time: 367 us -> 483 us (1.32)
  blocking collectives: 21.5 us -> 76.8 us
  waiting for transfers between devices: 237 us -> 282 us
  starting transfers between devices: 16.5 us -> 31 us
  local copies, waits for them, and re-layouts: 19.2 us -> 25.1 us
    all_to_all x0 -> x3, waiting for transfers between devices: none -> 107 us  [exchange_gather(): blocks = lax.all_to_all(blocks, name, split_axis=0, concat_axis=0)]
    all_to_all x0 -> x1, blocking collectives: none -> 76.8 us  [from_everyone(): return lax.all_to_all(copies, axis, split_axis=0, concat_axis=0, tiled=True)]
    all_gather x2 -> x0, waiting for transfers between devices: 66.9 us -> none  [gather_turned(): result, at, done = (lax.all_gather(both, axis, axis=0, tiled=True), 0, [])]
    all_gather x1 -> x0, blocking collectives: 21.5 us -> none  [gather_turned(): result, at, done = (lax.all_gather(both, axis, axis=0, tiled=True), 0, [])]
    all_to_all x0 -> x3, starting transfers between devices: none -> 19.8 us  [exchange_gather(): blocks = lax.all_to_all(blocks, name, split_axis=0, concat_axis=0)]
    all_to_all x3 -> x2, waiting for transfers between devices: 57.3 us -> 74.3 us  [from_everyone(): return lax.all_to_all(copies, axis, split_axis=0, concat_axis=0, tiled=True)]
    reduce_scatter x1, waiting for transfers between devices: 71.1 us -> 59.3 us  [shards(): lax.psum_scatter(jnp.dot(act, point_rows, preferred_element_type=jnp.floa...]
    another operation x0 -> x3, local copies, waits for them, and re-layouts: none -> 6.92 us  [exchange_gather(): blocks = jnp.stack([shard for _ in range(peers)])]
  transfers between devices with their start and end apart: 7 -> 7, of which waited for: 6 -> 6; matrix products, arithmetic and copies ran while one was open for 4% -> 7% of each run, Pallas kernels for 0% -> 0%
where the time goes in v1:
time: 483 us; the launch traced here: 482 us
  waiting for transfers between devices  282 us (58%)
  blocking collectives  76.8 us (16%)
  matrix products  41.6 us (9%)
  starting transfers between devices  31 us (6%)
  local copies, waits for them, and re-layouts  25.1 us (5%)
  between operations  13.7 us (3%)
  other arithmetic  12.3 us (3%)
    all_to_all x3, waiting for transfers between devices, exchange_gather(): blocks = lax.all_to_all(blocks, name, split_axis=0, concat_axis=0)  107 us
    all_to_all x1, blocking collectives, from_everyone(): return lax.all_to_all(copies, axis, split_axis=0, concat_axis=0, tiled=True)  76.8 us
    all_to_all x2, waiting for transfers between devices, from_everyone(): return lax.all_to_all(copies, axis, split_axis=0, concat_axis=0, tiled=True)  74.3 us
    reduce_scatter x1, waiting for transfers between devices, shards(): lax.psum_scatter(jnp.dot(act, point_rows, preferred_element_type=jnp.floa...  59.3 us
    reduce_scatter x1, waiting for transfers between devices, shards(): lax.psum_scatter((jnp.dot(hidden, down_part, preferred_element_type=jnp.f...  41.1 us
    all_to_all x3, starting transfers between devices, exchange_gather(): blocks = lax.all_to_all(blocks, name, split_axis=0, concat_axis=0)  19.8 us
    dot_general x1, matrix products, shards(): jnp.dot(hidden, down_part, preferred_element_type=jnp.float32) * down_full  19.4 us
    all_to_all x2, starting transfers between devices, from_everyone(): return lax.all_to_all(copies, axis, split_axis=0, concat_axis=0, tiled=True)  11.1 us
  transfers between devices with their start and end apart: 7, of which 6 were waited for; matrix products, arithmetic and copies ran while one was open for 7% of the time, Pallas kernels for 0%

profile of v1, /device:TPU:1, one launch (start us, length us, event | category | flops | bytes accessed | tf_op | source)
XLA Modules:
  0.0 481.9 jit_solution(14014560609665285897)
XLA Ops:
  6.5 0.9 convert_bitcast_fusion.1
  7.4 1.0 copy.44
  8.5 1.0 copy.43
  9.5 0.1 copy.45
  9.7 2.0 stack.6
  11.6 8.8 %all-to-all-start.1 = ((bf16[16,128,768]{2,1,0:T(8,128)(2,1)}), bf16[16,128,768]{2,1,0:T(8,128)(2,1)}, u32[]{:S(2)}, u32[]{:S(2)}) async-start(bf16[16,128,768]{2,1,0:T(8,128)(2,1)} %stack.6), calls=%async_computation.1 | async-start | bytes 6291456 | tf_op jit(solution)/shard_map/all_to_all | solution.py:12
  20.4 0.0 copy-done
  20.4 0.2 fusion.16
  20.6 0.0 copy-done.4
  20.7 0.3 fusion.18
  20.9 46.4 %all-to-all-done.1 = bf16[16,128,768]{2,1,0:T(8,128)(2,1)} async-done(((bf16[16,128,768]{2,1,0:T(8,128)(2,1)}), bf16[16,128,768]{2,1,0:T(8,128)(2,1)}, u32[]{:S(2)}, u32[]{:S(2)}) %all-to-all-start.1) | async-done | bytes 3145760 | tf_op jit(solution)/shard_map/all_to_all | solution.py:12
  67.3 3.4 broadcast_in_dim.6
  70.7 6.5 %all-to-all-start = ((bf16[8,192,2048]{2,1,0:T(8,128)(2,1)}), bf16[8,192,2048]{2,1,0:T(8,128)(2,1)}, u32[]{:S(2)}, u32[]{:S(2)}) async-start(bf16[8,192,2048]{2,1,0:T(8,128)(2,1)} %broadcast_in_dim.6), calls=%async_computation | async-start | bytes 12582912 | tf_op jit(solution)/shard_map/all_to_all | solution.py:35
  77.3 0.8 dynamic_slice.14
  78.0 0.8 dynamic_slice.13
  78.8 0.8 dynamic_slice.15
  79.6 0.0 copy-done.7
  79.6 1.2 fusion.68
  80.8 1.2 constant_dynamic-slice_fusion
  82.0 66.6 %all-to-all-done = bf16[8,192,2048]{2,1,0:T(8,128)(2,1)} async-done(((bf16[8,192,2048]{2,1,0:T(8,128)(2,1)}), bf16[8,192,2048]{2,1,0:T(8,128)(2,1)}, u32[]{:S(2)}, u32[]{:S(2)}) %all-to-all-start) | async-done | bytes 6291488 | tf_op jit(solution)/shard_map/all_to_all | solution.py:35
  148.6 0.6 stack.7
  149.2 4.1 all-to-all-start.3
  153.2 4.9 %fusion.14 = f32[1536,256]{1,0:T(8,128)S(1)} fusion(bf16[1536,2048]{1,0:T(8,128)(2,1)} %bitcast.1, bf16[2048,768]{1,0:T(8,128)(2,1)} %bitcast.3, f32[256]{0:T(256)S(1)} %dynamic_slice.14), kind=kOutput, calls=%fused_computation.18 | convolution fusion | flops 1612185600 | bytes 8913920 | tf_op jit(solution)/shard_map/dot_general | solution.py:113
  158.2 4.8 %fusion.15 = bf16[1536,256]{1,0:T(8,128)(2,1)S(1)} fusion(f32[1536,256]{1,0:T(8,128)S(1)} %fusion.14, bf16[1536,2048]{1,0:T(8,128)(2,1)} %bitcast.1, bf16[2048,768]{1,0:T(8,128)(2,1)} %bitcast.3, f32[256]{0:T(256)S(1)} %dynamic_slice.13), kind=kOutput, calls=%fused_computation.19 | convolution fusion | flops 1611792384 | bytes 9700352 | tf_op jit(solution)/shard_map/dot_general | solution.py:112
  163.0 0.2 pad_convert_fusion
  163.2 6.0 %fusion.24 = f32[1536,256]{1,0:T(8,128)S(1)} fusion(f32[1566,256]{1,0:T(8,128)S(1)} %pad_convert_fusion, f32[256]{0:T(256)S(1)} %bitcast.67, f32[256]{0:T(256)S(1)} %bitcast.69, f32[256]{0:T(256)S(1)} %bitcast.70, f32[256]{0:T(256)S(1)} %bitcast.71, f32[256]{0:T(256)S(1)} %bitcast.72, f32[256]{0:T(256)S(1)} %bitcast.73, f32[256]{0:T(256)S(1)} %bitcast.74, ...), kind=kLoop, calls=%fused_computation.35 | loop fusion | flops 23986176 | bytes 50363392 | tf_op jit(solution)/shard_map/add | solution.py:63
  169.2 1.8 fusion.54
  171.0 0.9 fusion.60
  171.9 1.6 reshape.101
  173.5 0.4 reshape.100
  173.9 0.0 all-to-all-done.3
  173.9 0.9 broadcast_in_dim.7
  174.9 4.6 all-to-all-start.2
  179.5 0.0 reduce-scatter.3.cloned.1.call-start
  179.5 7.7 %all-to-all-done.2 = f32[8,1,12288]{2,1,0:T(1,128)S(1)} async-done(((f32[8,1,12288]{2,1,0:T(1,128)}), f32[8,1,12288]{2,1,0:T(1,128)S(1)}, u32[]{:S(2)}, u32[]{:S(2)}) %all-to-all-start.2) | async-done | bytes 393248 | tf_op jit(solution)/shard_map/all_to_all | solution.py:35
  187.2 0.3 reduce_sum.28
  187.5 1.7 div.28
  189.2 0.8 div.26
  190.0 0.0 copy-start.1
  190.0 0.9 fusion.59
  190.9 0.3 copy-done.1
  191.1 1.3 multiply_convert_fusion.2
  192.5 7.6 %convolution_multiply_fusion = f32[1536,2048]{1,0:T(8,128)} fusion(bf16[1536,256]{1,0:T(8,128)(2,1)S(1)} %multiply_convert_fusion.2, f32[2048]{0:T(1024)S(1)} %bitcast.52, bf16[2048,768]{1,0:T(8,128)(2,1)} %bitcast.3), kind=kOutput, calls=%fused_computation.1 | convolution fusion | flops 1613758464 | bytes 14426112 | tf_op jit(solution)/shard_map/dot_general | solution.py:127
  200.1 0.0 reduce-scatter.3.cloned.1.call-update
  200.1 1.0 copy-done.2
  201.1 0.2 copy.49
  201.4 0.2 copy.50
  201.6 4.4 stack.8
  205.9 7.0 %all-to-all-start.5 = ((bf16[16,128,2048]{2,1,0:T(8,128)(2,1)}), bf16[16,128,2048]{2,1,0:T(8,128)(2,1)}, u32[]{:S(2)}, u32[]{:S(2)}) async-start(bf16[16,128,2048]{2,1,0:T(8,128)(2,1)} %stack.8), calls=%async_computation.6 | async-start | bytes 16777216 | tf_op jit(solution)/shard_map/all_to_all | solution.py:12
  212.9 0.0 copy-start.5
  213.0 0.0 reduce-scatter.5.cloned.1.call-start
  213.0 59.3 %reduce-scatter.3.cloned.1.call-done = f32[192,2048]{1,0:T(8,128)} async-done(((f32[1536,2048]{1,0:T(8,128)}), f32[192,2048]{1,0:T(8,128)}) %reduce-scatter.3.cloned.1.call-update) | async-done | bytes 1572880 | tf_op jit(solution)/shard_map/reduce_scatter | solution.py:126
  272.3 1.7 fusion.20
  274.0 0.0 copy-done.5
  274.0 0.3 fusion.22
  274.3 60.4 %all-to-all-done.5 = bf16[16,128,2048]{2,1,0:T(8,128)(2,1)} async-done(((bf16[16,128,2048]{2,1,0:T(8,128)(2,1)}), bf16[16,128,2048]{2,1,0:T(8,128)(2,1)}, u32[]{:S(2)}, u32[]{:S(2)}) %all-to-all-start.5) | async-done | bytes 8388640 | tf_op jit(solution)/shard_map/all_to_all | solution.py:12
  334.7 0.8 broadcast_in_dim.8
  335.5 0.0 copy-start.8
  335.5 76.8 %all_to_all.31 = bf16[8,192,2048]{2,1,0:T(8,128)(2,1)} all-to-all(bf16[8,192,2048]{2,1,0:T(8,128)(2,1)S(1)} %broadcast_in_dim.8), channel_id=1, replica_groups=mesh['fs'=16,'tp'=8] {'tp'}, dimensions={0} | all-to-all | bytes 12582912 | tf_op jit(solution)/shard_map/all_to_all | solution.py:35
  412.3 0.0 copy-done.8
  412.3 19.4 %multiply_convert_fusion = bf16[1536,2048]{1,0:T(8,128)(2,1)} fusion(f32[2048]{0:T(1024)S(1)} %bitcast.54, bf16[2048,2048]{1,0:T(8,128)(2,1)} %bitcast.40, bf16[1536,2048]{1,0:T(8,128)(2,1)} %bitcast.51, f32[1024]{0:T(1024)S(1)} %copy-done.8), kind=kOutput, calls=%fused_computation | convolution fusion | flops 12897484800 | bytes 20983808 | tf_op jit(solution)/shard_map/dot_general | solution.py:141
  431.7 0.0 reduce-scatter.5.cloned.1.call-update
  431.7 41.1 %reduce-scatter.5.cloned.1.call-done = bf16[192,2048]{1,0:T(8,128)(2,1)} async-done(((bf16[1536,2048]{1,0:T(8,128)(2,1)}), bf16[192,2048]{1,0:T(8,128)(2,1)}) %reduce-scatter.5.cloned.1.call-update) | async-done | bytes 786448 | tf_op jit(solution)/shard_map/reduce_scatter | solution.py:140
  472.8 2.3 fusion.23
  (18 shorter events, 0.2 us)
Async XLA Ops:
  11.6 8.8 %copy-start = (bf16[192,2048]{1,0:T(8,128)(2,1)S(1)}, bf16[192,2048]{1,0:T(8,128)(2,1)}, u32[]{:S(2)}) copy-start(bf16[192,2048]{1,0:T(8,128)(2,1)} %param.15) | copy-start | bytes 2359300
  11.6 9.0 %copy-start.4 = (f32[2048]{0:T(1024)S(1)}, f32[2048]{0:T(1024)}, u32[]{:S(2)}) copy-start(f32[2048]{0:T(1024)} %param.16) | copy-start | bytes 24580
  11.6 55.7 %all-to-all-start.1 = ((bf16[16,128,768]{2,1,0:T(8,128)(2,1)}), bf16[16,128,768]{2,1,0:T(8,128)(2,1)}, u32[]{:S(2)}, u32[]{:S(2)}) async-start(bf16[16,128,768]{2,1,0:T(8,128)(2,1)} %stack.6), calls=%async_computation.1 | async-start | bytes 6291456 | tf_op jit(solution)/shard_map/all_to_all | solution.py:12
  70.7 8.8 %copy-start.6 = (f32[128]{0:T(128)S(1)}, f32[128]{0:T(128)}, u32[]{:S(2)}) copy-start(f32[128]{0:T(128)} %param.29) | copy-start | bytes 1540
  70.7 8.8 %copy-start.7 = (f32[128]{0:T(128)S(1)}, f32[128]{0:T(128)}, u32[]{:S(2)}) copy-start(f32[128]{0:T(128)} %param.24) | copy-start | bytes 1540
  70.7 77.8 %all-to-all-start = ((bf16[8,192,2048]{2,1,0:T(8,128)(2,1)}), bf16[8,192,2048]{2,1,0:T(8,128)(2,1)}, u32[]{:S(2)}, u32[]{:S(2)}) async-start(bf16[8,192,2048]{2,1,0:T(8,128)(2,1)} %broadcast_in_dim.6), calls=%async_computation | async-start | bytes 12582912 | tf_op jit(solution)/shard_map/all_to_all | solution.py:35
  149.2 24.8 %all-to-all-start.3 = ((f32[16,128,2]{1,2,0:T(2,128)}), f32[16,128,2]{1,2,0:T(2,128)S(1)}, u32[]{:S(2)}, u32[]{:S(2)}) async-start(f32[16,128,2]{1,2,0:T(2,128)} %stack.7), calls=%async_computation.3 | async-start | bytes 32768 | tf_op jit(solution)/shard_map/all_to_all | solution.py:12
  174.9 12.3 %all-to-all-start.2 = ((f32[8,1,12288]{2,1,0:T(1,128)}), f32[8,1,12288]{2,1,0:T(1,128)S(1)}, u32[]{:S(2)}, u32[]{:S(2)}) async-start(f32[8,1,12288]{2,1,0:T(1,128)} %broadcast_in_dim.7), calls=%async_computation.2 | async-start | bytes 786432 | tf_op jit(solution)/shard_map/all_to_all | solution.py:35
  179.5 92.8 %reduce-scatter.3.cloned.1.call-start = ((), (), s32[]{:S(2)}) async-start(), calls=%async_computation.8 | async-start | bytes 14155776 | tf_op jit(solution)/shard_map/reduce_scatter | solution.py:126
  190.0 1.1 copy-start.1
  200.1 1.0 copy-start.2
  200.1 1.2 copy-start.3
  205.9 128.8 %all-to-all-start.5 = ((bf16[16,128,2048]{2,1,0:T(8,128)(2,1)}), bf16[16,128,2048]{2,1,0:T(8,128)(2,1)}, u32[]{:S(2)}, u32[]{:S(2)}) async-start(bf16[16,128,2048]{2,1,0:T(8,128)(2,1)} %stack.8), calls=%async_computation.6 | async-start | bytes 16777216 | tf_op jit(solution)/shard_map/all_to_all | solution.py:12
  212.9 61.1 %copy-start.5 = (f32[2048]{0:T(1024)S(1)}, f32[2048]{0:T(1024)}, u32[]{:S(2)}) copy-start(f32[2048]{0:T(1024)} %param.25) | copy-start | bytes 24580
  213.0 259.9 %reduce-scatter.5.cloned.1.call-start = ((), (), s32[]{:S(2)}) async-start(), calls=%async_computation.9 | async-start | bytes 7077888 | tf_op jit(solution)/shard_map/reduce_scatter | solution.py:140
  335.5 76.8 %copy-start.8 = (f32[1024]{0:T(1024)S(1)}, f32[1024]{0:T(1024)}, u32[]{:S(2)}) copy-start(f32[1024]{0:T(1024)} %param.27) | copy-start | bytes 12292
Sparse Core Ops, SparseCore 0:
  200.2 72.0 reduce-scatter.2
  431.8 40.9 reduce-scatter.4
